TPU v7x, 32 devices: a whole 2x2x4 slice. The times are simulated.
32 devices in a mesh: kv: 8 (over z, y), tp: 4 (over x, core).
Axes of the slice: x: 2, y: 2, z: 4, core: 2. Of those that a mesh axis runs over, the one named last changes fastest.
Arguments:
- tokens: bfloat16 [2048, 2048], P('kv'), may hold values from -6 to 6
- query_weight: bfloat16 [2048, 2048], P(None, 'tp'), may hold values from -0.125 to 0.125
- key_weight: bfloat16 [2048, 512], P(None, 'tp'), may hold values from -0.125 to 0.125
- value_weight: bfloat16 [2048, 512], P(None, 'tp'), may hold values from -0.125 to 0.125
- gate_weight: bfloat16 [2048, 64], replicated, may hold values from -0.125 to 0.125
- query_gain: float32 [64], replicated
- key_gain: float32 [64], replicated
- out_weight: bfloat16 [2048, 2048], P('tp'), may hold values from -0.125 to 0.125
- shared_block: int32 [8], P('kv'), may hold values from 0 to 3, as said below
- chosen_device: int32 [32, 7], P('kv'), may hold values from 0 to 7, as said below
Outputs:
- mixed_out: bfloat16 [2048, 2048], P(('kv', 'tp'))
- log_weight: float32 [2, 2048, 32], P(None, 'kv', 'tp')
Inputs may be any that keep to these rules, and one draw needn't show every extreme that they name: `shared_block`: entry d names one of the 64-position blocks of device d's 256 positions. `chosen_device`: row b names 7 different devices, never the device that holds query block b.
All inputs are finite; a program needn't handle non-finite values.
Results may differ from a plain program's by a relative error of at most 0.019.
The roundings to bfloat16 on the way count: a program that leaves them out, or rounds other values in their place, can miss the bound.
Values may be sent and summed in bfloat16 or wider, within the bound.
A program may use at most 64 MiB of HBM per device.

v0:
```python
import math

import jax
import jax.numpy as jnp
from jax import lax
from jax.sharding import PartitionSpec as P

SEL = 64
CMP = 32


norm_eps = 1e-06
rope_base = 500000.0
big_negative = -1e30


def rounded(values_in):
    return lax.optimization_barrier(values_in.astype(jnp.bfloat16))


def unit_norm(values_in, gain_vec):
    upcast = values_in.astype(jnp.float32)
    return (
        upcast * lax.rsqrt(jnp.mean(upcast * upcast, axis=-1, keepdims=True) + norm_eps) * gain_vec
    )


def rotate(values_in, places):
    half_size = values_in.shape[-1] // 2
    inverse = jnp.power(
        rope_base, -jnp.arange(half_size, dtype=jnp.float32) * 2.0 / values_in.shape[-1]
    )
    angles = places.astype(jnp.float32)[:, None] * inverse[None, :]
    cos_vals = jnp.cos(angles)[:, None, :]
    sin_vals = jnp.sin(angles)[:, None, :]
    upcast = values_in.astype(jnp.float32)
    front_half = upcast[..., :half_size]
    back_half = upcast[..., half_size:]
    return jnp.concatenate(
        [
            front_half * cos_vals - back_half * sin_vals,
            back_half * cos_vals + front_half * sin_vals,
        ],
        axis=-1,
    )


def shards(
    tokens,
    query_weight,
    key_weight,
    value_weight,
    gate_weight,
    query_gain,
    key_gain,
    out_weight,
    shared_block,
    chosen_device,
):
    tok_rows = tokens.shape[0]
    head_size = query_gain.shape[0]
    head_count = query_weight.shape[1] // head_size
    groups = key_weight.shape[1] // head_size
    per_group = head_count // groups
    group_width = groups * head_size
    block_len = SEL
    local_blocks = tok_rows // block_len
    device = lax.axis_index("kv")
    tp_index = lax.axis_index("tp")
    score_scale = head_size ** (-0.5)
    places = device * tok_rows + jnp.arange(tok_rows, dtype=jnp.int32)
    queries = rounded(jnp.dot(tokens, query_weight, preferred_element_type=jnp.float32)).reshape(
        tok_rows, head_count, head_size
    )
    keys_raw = rounded(jnp.dot(tokens, key_weight, preferred_element_type=jnp.float32)).reshape(
        tok_rows, groups, head_size
    )
    values_raw = rounded(jnp.dot(tokens, value_weight, preferred_element_type=jnp.float32))
    q_plain = rounded(unit_norm(queries, query_gain))
    k_plain = rounded(unit_norm(keys_raw, key_gain))
    q_turned = rotate(q_plain, places).astype(jnp.bfloat16)
    k_turned = rotate(k_plain, places).astype(jnp.bfloat16).reshape(tok_rows, group_width)
    gate_cols = lax.dynamic_slice_in_dim(gate_weight, tp_index * 2 * head_count, 2 * head_count, 1)
    gate_vals = jax.nn.sigmoid(
        jnp.dot(tokens, gate_cols, preferred_element_type=jnp.float32)
    ).reshape(tok_rows, head_count, 2)
    span_count = tok_rows // CMP
    span_keys = jnp.mean(
        k_plain.astype(jnp.float32).reshape(span_count, CMP, group_width), axis=1
    ).astype(jnp.bfloat16)
    span_values = jnp.mean(
        values_raw.astype(jnp.float32).reshape(span_count, CMP, group_width), axis=1
    ).astype(jnp.bfloat16)
    summary = jnp.concatenate([span_keys, span_values], axis=1)
    first_row = shared_block[0] * block_len
    shared = jnp.concatenate(
        [
            lax.dynamic_slice_in_dim(k_turned, first_row, block_len, 0),
            lax.dynamic_slice_in_dim(values_raw, first_row, block_len, 0),
        ],
        axis=1,
    )[None]
    all_summary = lax.all_gather(summary, "kv", axis=0, tiled=True)
    total_spans = all_summary.shape[0]
    span_keys_all = all_summary[:, :group_width].reshape(total_spans, groups, head_size)
    span_values_all = all_summary[:, group_width:].reshape(total_spans, groups, head_size)
    q_grouped = q_plain.reshape(tok_rows, groups, per_group, head_size)
    scores = (
        jnp.einsum("rghd,cgd->rghc", q_grouped, span_keys_all, preferred_element_type=jnp.float32)
        * score_scale
    )
    span_ends = jnp.arange(total_spans, dtype=jnp.int32) * CMP + CMP - 1
    allowed = (span_ends[None, :] <= places[:, None])[:, None, None, :]
    has_span = (places >= CMP - 1)[:, None, None]
    peak_val = jnp.max(jnp.where(allowed, scores, big_negative), axis=-1)
    weights_raw = jnp.where(allowed, jnp.exp(scores - peak_val[..., None]), 0.0)
    divisor = jnp.where(has_span, jnp.sum(weights_raw, axis=-1), 1.0)
    span_out = (
        jnp.einsum(
            "rghc,cgd->rghd",
            weights_raw.astype(jnp.bfloat16),
            span_values_all,
            preferred_element_type=jnp.float32,
        )
        / divisor[..., None]
    )
    span_lse = jnp.where(has_span, peak_val + jnp.log(divisor), 0.0)
    q_blocks = q_turned.reshape(local_blocks, block_len, groups, per_group, head_size)
    own_keys = k_turned.reshape(local_blocks, block_len, groups, head_size)
    own_values = values_raw.reshape(local_blocks, block_len, groups, head_size)
    causal_own = jnp.arange(block_len)[None, :] <= jnp.arange(block_len)[:, None]
    device_ids = jnp.arange(lax.axis_size("kv"), dtype=jnp.int32)
    member = jnp.any(chosen_device[:, :, None] == device_ids[None, None, :], axis=1) & (
        device_ids[None, :] < device
    )
    own_allowed = causal_own[None, :, None, None, :]
    own_scores = (
        jnp.einsum("jqghd,jkgd->jqghk", q_blocks, own_keys, preferred_element_type=jnp.float32)
        * score_scale
    )
    peak_own = jnp.max(jnp.where(own_allowed, own_scores, big_negative), axis=-1)
    weights_own = jnp.where(own_allowed, jnp.exp(own_scores - peak_own[..., None]), 0.0)
    running = (
        peak_own,
        jnp.sum(weights_own, axis=-1),
        jnp.einsum(
            "jqghk,jkgd->jqghd",
            weights_own.astype(jnp.bfloat16),
            own_values,
            preferred_element_type=jnp.float32,
        ),
    )
    fold_state = running
    gathered_piece = lax.all_gather(shared, "kv", axis=0, tiled=True)
    row_count = gathered_piece.shape[0]
    stride = math.gcd(row_count, 8)
    slab_list = gathered_piece.reshape(row_count // stride, stride * block_len, 2 * group_width)
    slab_flags = member.reshape(local_blocks, row_count // stride, stride).transpose(1, 0, 2)

    def absorb_slab(inner_state, inputs):
        slab_rows, slab_flag = inputs
        old_peak, old_sum, weighted = inner_state
        slab_keys = slab_rows[:, :group_width].reshape(-1, groups, head_size)
        slab_values = slab_rows[:, group_width:].reshape(-1, groups, head_size)
        counted = jnp.repeat(slab_flag, block_len, axis=1)[:, None, None, None, :]
        scores_slab = (
            jnp.einsum("jqghd,kgd->jqghk", q_blocks, slab_keys, preferred_element_type=jnp.float32)
            * score_scale
        )
        new_peak = jnp.maximum(
            old_peak, jnp.max(jnp.where(counted, scores_slab, big_negative), axis=-1)
        )
        factor = jnp.exp(old_peak - new_peak)
        weights_slab = jnp.where(counted, jnp.exp(scores_slab - new_peak[..., None]), 0.0)
        new_weighted = weighted * factor[..., None] + jnp.einsum(
            "jqghk,kgd->jqghd",
            weights_slab.astype(jnp.bfloat16),
            slab_values,
            preferred_element_type=jnp.float32,
        )
        return ((new_peak, old_sum * factor + jnp.sum(weights_slab, axis=-1), new_weighted), None)

    fold_state, ignored = lax.scan(absorb_slab, fold_state, (slab_list, slab_flags))
    peak_sel, sum_sel, weighted = fold_state
    chosen_out = weighted / sum_sel[..., None]
    chosen_lse = peak_sel + jnp.log(sum_sel)
    mixed_heads = (
        gate_vals[..., 0:1] * span_out.reshape(tok_rows, head_count, head_size)
        + gate_vals[..., 1:2] * chosen_out.reshape(tok_rows, head_count, head_size)
    ).astype(jnp.bfloat16)
    mixed_heads = mixed_heads.reshape(tok_rows, head_count * head_size)
    mixed_out = lax.psum_scatter(
        jnp.dot(mixed_heads, out_weight, preferred_element_type=jnp.float32).astype(jnp.bfloat16),
        "tp",
        scatter_dimension=0,
        tiled=True,
    )
    log_weight = jnp.stack(
        [span_lse.reshape(tok_rows, head_count), chosen_lse.reshape(tok_rows, head_count)]
    )
    return (mixed_out, log_weight)


def solution(mesh):
    placed = (
        P("kv", None),
        P(None, "tp"),
        P(None, "tp"),
        P(None, "tp"),
        P(),
        P(),
        P(),
        P("tp", None),
        P("kv"),
        P("kv", None),
    )
    return jax.shard_map(
        shards,
        mesh=mesh,
        in_specs=placed,
        out_specs=(P(("kv", "tp"), None), P(None, "kv", "tp")),
        check_vma=False,
    )
```

profile of v0, /device:TPU:17, one launch (start us, length us, event | category | flops | bytes accessed | tf_op | source)
XLA Modules:
  0.0 152.0 jit_solution(13710061051719848535)
XLA Ops:
  7.3 2.0 %convolution_convert_fusion.3 = bf16[256,128]{1,0:T(8,128)(2,1)S(1)} fusion(bf16[256,2048]{1,0:T(8,128)(2,1)} %param.10, bf16[2048,128]{1,0:T(8,128)(2,1)} %param.12), kind=kOutput, calls=%fused_computation.23 | convolution fusion | flops 134250496 | bytes 1638400 | tf_op jit(solution)/shard_map/dot_general | solution.py:75
  12.3 1.5 convolution_convert_fusion.2
  17.9 2.3 %convolution_convert_fusion.1 = bf16[256,512]{1,0:T(8,128)(2,1)S(1)} fusion(bf16[256,2048]{1,0:T(8,128)(2,1)S(1)} %copy-done.1, bf16[2048,512]{1,0:T(8,128)(2,1)} %param.11), kind=kOutput, calls=%fused_computation.21 | convolution fusion | flops 537001984 | bytes 3407872 | tf_op jit(solution)/shard_map/dot_general | solution.py:72
  20.2 0.9 copy.146
  21.2 1.1 multiply_reduce_fusion
  22.3 1.1 multiply_convert_fusion
  24.3 1.8 %concatenate.32 = bf16[4,64,2,4,32]{1,0,4,3,2:T(4,128)(2,1)} reshape(bf16[256,8,32]{0,2,1:T(8,128)(2,1)} %get-tuple-element.28) | data formatting | bytes 262144 | tf_op jit(solution)/shard_map/concatenate | solution.py:39
  26.1 2.0 %copy.151 = bf16[4,64,2,4,32]{4,1,3,2,0:T(8,128)(2,1)} copy(bf16[4,64,2,4,32]{1,0,4,3,2:T(4,128)(2,1)} %concatenate.32) | data formatting | bytes 262144 | tf_op jit(solution)/shard_map/concatenate | solution.py:39
  28.0 1.8 %concatenate.31 = bf16[4,64,2,4,32]{1,0,4,3,2:T(4,128)(2,1)} reshape(bf16[256,8,32]{0,2,1:T(8,128)(2,1)} %get-tuple-element.20) | data formatting | bytes 262144 | tf_op jit(solution)/shard_map/concatenate | solution.py:39
  29.8 2.0 %copy.150 = bf16[4,64,2,4,32]{4,1,3,2,0:T(8,128)(2,1)} copy(bf16[4,64,2,4,32]{1,0,4,3,2:T(4,128)(2,1)} %concatenate.31) | data formatting | bytes 262144 | tf_op jit(solution)/shard_map/concatenate | solution.py:39
  34.2 0.8 constant_dynamic-slice_fusion.1
  35.1 20.7 %all-gather = bf16[512,256]{1,0:T(8,128)(2,1)S(1)} all-gather(bf16[64,256]{1,0:T(8,128)(2,1)S(1)} %pad_maximum_fusion.2), channel_id=2, replica_groups=mesh['kv'=8,'tp'=4] {'kv'}, dimensions={0}, use_global_device_ids=true | all-gather | bytes 294912 | tf_op jit(solution)/shard_map/all_gather | solution.py:154
  56.6 1.0 copy.156
  57.6 1.7 %copy.159 = bf16[512,128]{0,1:T(8,128)(2,1)} copy(bf16[512,128]{1,0:T(8,128)(2,1)} %get-tuple-element.29) | data formatting | bytes 262144 | tf_op jit(solution)/shard_map/while/body/eval_jaxpr/slice | solution.py:164
  59.3 2.2 %fusion = (f32[4,64,2,4]{1,3,0,2:T(4,128)S(1)}, f32[2,512,4,64,4]{1,3,4,2,0:T(8,128)S(1)}) fusion(pred[4,512]{1,0:T(4,128)(4,1)S(1)} %broadcast_in_dim.131, bf16[512,2,64,1,1]{0,2,4,3,1:T(8,128)(2,1)S(1)} %bitcast.125, bf16[4,64,2,4,32]{4,1,3,2,0:T(8,128)(2,1)} %copy.151, bf16[4,64,2,4,32]{4,1,3,2,0:T(8,128)(2,1)} %copy.150), kind=kOutput, calls=%fused_computation.2 | convolution fusion | flops 137885696 | bytes 4597760 | tf_op jit(solution)/shard_map/while/body/eval_jaxpr/jqghd,kgd->jqghk/dot_general | solution.py:167
  62.5 1.1 fusion.4
  64.6 1.1 fusion.15
  65.7 1.7 %copy.180 = f32[4,64,2,4,64]{1,0,4,3,2:T(4,128)} copy(f32[4,64,2,4,64]{1,4,3,2,0:T(8,128)S(1)} %fusion.15) | data formatting | bytes 1048576 | tf_op jit(solution)/shard_map/reshape | solution.py:189
  67.4 2.7 %reshape.358 = f32[256,512]{0,1:T(8,128)} reshape(f32[4,64,2,4,64]{1,0,4,3,2:T(4,128)} %copy.180) | data formatting | bytes 1048576 | tf_op jit(solution)/shard_map/reshape | solution.py:189
  70.7 1.1 reshape.335
  73.8 23.9 %all_gather.6 = bf16[64,256]{1,0:T(8,128)(2,1)S(1)} all-gather(bf16[8,256]{1,0:T(8,128)(2,1)S(1)} %pad_maximum_fusion.4), channel_id=1, replica_groups=mesh['kv'=8,'tp'=4] {'kv'}, dimensions={0}, use_global_device_ids=true | all-gather | bytes 36864 | tf_op jit(solution)/shard_map/all_gather | solution.py:103
  97.9 1.2 fusion.23
  100.7 1.7 %convolution_convert_fusion = bf16[256,2048]{1,0:T(8,128)(2,1)} fusion(bf16[256,512]{0,1:T(8,128)(2,1)S(1)} %fusion.28, bf16[512,2048]{1,0:T(8,128)(2,1)S(1)} %copy-done), kind=kOutput, calls=%fused_computation.7 | convolution fusion | flops 537395200 | bytes 3407872 | tf_op jit(solution)/shard_map/dot_general | solution.py:193
  103.6 41.5 %reduce-scatter.2.cloned.1.call-done = bf16[64,2048]{1,0:T(8,128)(2,1)} async-done(((bf16[256,2048]{1,0:T(8,128)(2,1)}), bf16[64,2048]{1,0:T(8,128)(2,1)}) %reduce-scatter.2.cloned.1.call-update) | async-done | bytes 262160 | tf_op jit(solution)/shard_map/reduce_scatter | solution.py:192
  (102 shorter events, 17.8 us)
Async XLA Ops:
  7.2 93.5 %copy-start = (bf16[512,2048]{1,0:T(8,128)(2,1)S(1)}, bf16[512,2048]{1,0:T(8,128)(2,1)}, u32[]{:S(2)}) copy-start(bf16[512,2048]{1,0:T(8,128)(2,1)} %param.17) | copy-start | bytes 6291460
  7.2 5.2 %copy-start.1 = (bf16[256,2048]{1,0:T(8,128)(2,1)S(1)}, bf16[256,2048]{1,0:T(8,128)(2,1)}, u32[]{:S(2)}) copy-start(bf16[256,2048]{1,0:T(8,128)(2,1)} %param.10) | copy-start | bytes 3145732
  7.2 137.9 %reduce-scatter.2.cloned.1.call-start = ((), (), s32[]{:S(2)}) async-start(), calls=%async_computation.1 | async-start | bytes 1310720 | tf_op jit(solution)/shard_map/reduce_scatter | solution.py:192
  17.9 4.4 %copy-start.16 = (f32[64]{0:T(128)S(1)}, f32[64]{0:T(128)}, u32[]{:S(2)}) copy-start(f32[64]{0:T(128)} %param.15) | copy-start | bytes 772
  59.3 2.2 %copy-start.2 = (bf16[4,64,2,4,32]{4,1,3,2,0:T(8,128)(2,1)S(1)}, bf16[4,64,2,4,32]{4,1,3,2,0:T(8,128)(2,1)}, u32[]{:S(2)}) copy-start(bf16[4,64,2,4,32]{4,1,3,2,0:T(8,128)(2,1)} %copy.151) | copy-start | bytes 393220
  59.3 2.2 %copy-start.3 = (bf16[4,64,2,4,32]{4,1,3,2,0:T(8,128)(2,1)S(1)}, bf16[4,64,2,4,32]{4,1,3,2,0:T(8,128)(2,1)}, u32[]{:S(2)}) copy-start(bf16[4,64,2,4,32]{4,1,3,2,0:T(8,128)(2,1)} %copy.150) | copy-start | bytes 393220
  59.3 2.2 %copy-start.6 = (bf16[4,64,2,32]{3,1,2,0:T(8,128)(2,1)S(1)}, bf16[4,64,2,32]{3,1,2,0:T(8,128)(2,1)}, u32[]{:S(2)}) copy-start(bf16[4,64,2,32]{3,1,2,0:T(8,128)(2,1)} %copy.149) | copy-start | bytes 98308
  59.3 2.2 %copy-start.7 = (bf16[4,64,2,32]{3,1,2,0:T(8,128)(2,1)S(1)}, bf16[4,64,2,32]{3,1,2,0:T(8,128)(2,1)}, u32[]{:S(2)}) copy-start(bf16[4,64,2,32]{3,1,2,0:T(8,128)(2,1)} %copy.148) | copy-start | bytes 98308
  61.5 2.2 %copy-start.8 = (f32[4,64,2,4]{1,3,0,2:T(4,128)}, f32[4,64,2,4]{1,3,0,2:T(4,128)S(1)}, u32[]{:S(2)}) copy-start(f32[4,64,2,4]{1,3,0,2:T(4,128)S(1)} %get-tuple-element.41) | copy-start | bytes 24580
  62.5 1.2 copy-start.10
  62.5 1.2 copy-start.5
  63.7 2.0 %copy-start.12 = (f32[4,64,2,4]{1,3,0,2:T(4,128)}, f32[4,64,2,4]{1,3,0,2:T(4,128)S(1)}, u32[]{:S(2)}) copy-start(f32[4,64,2,4]{1,3,0,2:T(4,128)S(1)} %get-tuple-element.19) | copy-start | bytes 24580
  63.7 0.9 copy-start.14
  72.4 27.9 %copy-start.15 = (pred[256]{0:T(512)(128)(4,1)S(1)}, pred[256]{0:T(512)(128)(4,1)}, u32[]{:S(2)}) copy-start(pred[256]{0:T(512)(128)(4,1)} %fusion.48) | copy-start | bytes 772
  99.1 1.5 copy-start.4
  100.7 1.8 %copy-start.13 = (f32[4,64,2,4]{1,3,0,2:T(4,128)S(1)}, f32[4,64,2,4]{1,3,0,2:T(4,128)}, u32[]{:S(2)}) copy-start(f32[4,64,2,4]{1,3,0,2:T(4,128)} %copy-done.12) | copy-start | bytes 24580
  100.7 1.8 %copy-start.11 = (f32[4,64,2,4]{1,3,2,0:T(4,128)S(1)}, f32[4,64,2,4]{1,3,2,0:T(4,128)}, u32[]{:S(2)}) copy-start(f32[4,64,2,4]{1,3,2,0:T(4,128)} %copy-done.10) | copy-start | bytes 24580
  100.7 1.8 %copy-start.9 = (f32[4,64,2,4]{1,3,0,2:T(4,128)S(1)}, f32[4,64,2,4]{1,3,0,2:T(4,128)}, u32[]{:S(2)}) copy-start(f32[4,64,2,4]{1,3,0,2:T(4,128)} %copy-done.8) | copy-start | bytes 24580
Sparse Core Ops, SparseCore 0:
  102.6 42.4 reduce-scatter.1
where the time goes:
time: 155 us; the launch traced here: 152 us
  blocking collectives  44.6 us (29%)
  waiting for transfers between devices  41.6 us (27%)
  local copies, waits for them, and re-layouts  23.8 us (15%)
  between operations  15.2 us (10%)
  matrix products  13.5 us (9%)
  other arithmetic  13.2 us (9%)
    reduce_scatter x1, waiting for transfers between devices, shards(): lax.psum_scatter(jnp.dot(mixed_heads, out_weight, preferred_element_type=...  41.5 us
    all_gather x1, blocking collectives, shards(): all_summary = lax.all_gather(summary, 'kv', axis=0, tiled=True)  23.9 us
    all_gather x1, blocking collectives, shards(): gathered_piece = lax.all_gather(shared, 'kv', axis=0, tiled=True)  20.7 us
    concatenate x8, local copies, waits for them, and re-layouts, rotate(): jnp.concatenate([front_half * cos_vals - back_half * sin_vals, back_half...  9.29 us
    reshape x2, local copies, waits for them, and re-layouts, shards(): chosen_out.reshape(tok_rows, head_count, head_size)  4.33 us
  transfers between devices with their start and end apart: 1, of which 1 were waited for; matrix products, arithmetic and copies ran while one was open for 1% of the time, Pallas kernels for 0%

commit v1 on v0

v1 whole, which is shorter than its diff:
```python
import functools

import jax
import jax.numpy as jnp
import numpy as np
from jax import lax
from jax.experimental import pallas as pl
from jax.experimental.pallas import tpu as pltpu
from jax.sharding import PartitionSpec as P

SEL = 64
CMP = 32
LANES = 128
SPAN_PAD = 16

norm_eps = 1e-06
rope_base = 500000.0
big_negative = -1e30

F32 = jnp.float32
BF16 = jnp.bfloat16
MESH = pl.DeviceIdType.MESH


def mm(a, b):
    return lax.dot_general(a, b, (((1,), (0,)), ((), ())), preferred_element_type=F32)


def mm_t(a, b):
    return lax.dot_general(a, b, (((1,), (1,)), ((), ())), preferred_element_type=F32)


def iota(shape, dim):
    return lax.broadcasted_iota(jnp.int32, shape, dim)


def tile_lanes(row, times):
    return row if times == 1 else jnp.concatenate([row] * times, axis=1)


def layer_kernel(
    n_kv, n_tp, heads, groups, head_size,
    tok_hbm, wq_hbm, wk_hbm, wv_hbm, wg_hbm, wo_hbm, tab_hbm, base_hbm,
    qgain_ref, kgain_ref, shared_ref, chosen_ref,
    out_ref, lse_ref,
    tok, wq, wkv, wg, wo, tab, base,
    own, slab, gath, qp_heads, qt_heads, gates, mixed, lse_rows,
    pair_send, pair_recv, cross_send, cross_recv,
    load_sem, slab_ss, slab_rs, pair_ss, pair_rs, cross_ss, cross_rs,
):
    rows = tok.shape[0]
    per_group = heads // groups
    half = LANES // 2
    n_x = n_tp // 2
    chunk = rows // n_tp
    n_chosen = chosen_ref.shape[1]
    me = lax.axis_index("kv")
    my_tp = lax.axis_index("tp")
    my_x = my_tp // 2
    my_core = my_tp % 2

    loads = [
        pltpu.make_async_copy(src, dst, load_sem.at[i])
        for i, (src, dst) in enumerate([
            (tok_hbm, tok),
            (wk_hbm, wkv.at[:, 0:LANES]),
            (wv_hbm, wkv.at[:, LANES:2 * LANES]),
            (tab_hbm, tab),
            (base_hbm, base),
            (wq_hbm, wq),
            (wg_hbm, wg),
            (wo_hbm, wo),
        ])
    ]
    for copy in loads:
        copy.start()

    barrier = pltpu.get_barrier_semaphore()

    def greet_kv(d, carry):
        @pl.when(d != me)
        def _():
            pl.semaphore_signal(barrier, inc=1, device_id={"kv": d}, device_id_type=MESH)
        return carry

    lax.fori_loop(0, n_kv, greet_kv, 0)
    for t in range(1, n_tp):
        peer = lax.rem(my_tp + t, n_tp)
        pl.semaphore_signal(barrier, inc=1, device_id={"tp": peer}, device_id_type=MESH)

    def clear(d, carry):
        gath[d] = jnp.zeros(gath.shape[1:], BF16)
        return carry

    lax.fori_loop(me + 1, n_kv, clear, 0)

    big = 2 * LANES
    row_i = iota((big, big), 0)
    col_i = iota((big, big), 1)
    block_mean = jnp.where(row_i // head_size == col_i // head_size, 1.0 / head_size, 0.0).astype(BF16)
    hs2 = head_size // 2
    first = (col_i % head_size) < hs2
    swap = jnp.where(
        first & (row_i == col_i + hs2), -1.0,
        jnp.where((~first) & (row_i == col_i - hs2), 1.0, 0.0),
    ).astype(BF16)

    def by_tiles(x, mat):
        width = x.shape[1]
        step = min(width, big)
        parts = [mm(x[:, i:i + step], mat[:step, :step]) for i in range(0, width, step)]
        return parts[0] if len(parts) == 1 else jnp.concatenate(parts, axis=1)

    def unit_norm(x, gain_row):
        sq = x * x
        hi = sq.astype(BF16)
        lo = (sq - hi.astype(F32)).astype(BF16)
        mean = by_tiles(hi, block_mean) + by_tiles(lo, block_mean)
        return (x * lax.rsqrt(mean + norm_eps) * gain_row).astype(BF16)

    loads[3].wait()
    loads[4].wait()
    cos_b = base[0, pl.ds(me, 1), :]
    sin_b = base[1, pl.ds(me, 1), :]
    cos_t = tab[0] * cos_b - tab[1] * sin_b
    sin_t = tab[1] * cos_b + tab[0] * sin_b

    def rotate(x):
        times = x.shape[1] // LANES
        return x.astype(F32) * tile_lanes(cos_t, times) + by_tiles(x, swap) * tile_lanes(sin_t, times)

    loads[0].wait()
    loads[1].wait()
    loads[2].wait()
    tokens = tok[...]
    kv_raw = mm(tokens, wkv[...]).astype(BF16)
    values = kv_raw[:, LANES:]
    k_gain = tile_lanes(kgain_ref[...], LANES // head_size)
    k_plain = unit_norm(kv_raw[:, :LANES].astype(F32), k_gain)
    k_turned = rotate(k_plain).astype(BF16)
    own[:, :LANES] = k_turned
    own[:, LANES:] = values
    spans_dev = rows // CMP
    avg = jnp.where(
        iota((SPAN_PAD, rows), 1) // CMP == iota((SPAN_PAD, rows), 0), 1.0 / CMP, 0.0
    ).astype(BF16)
    summary_k = mm(avg, k_plain).astype(BF16)
    summary_v = mm(avg, values).astype(BF16)
    slab[SEL:, :LANES] = summary_k
    slab[SEL:, LANES:] = summary_v
    gath[me, SEL:, :LANES] = summary_k
    gath[me, SEL:, LANES:] = summary_v
    pick = iota((SEL, rows), 1) == iota((SEL, rows), 0) + shared_ref[0] * SEL
    pick = jnp.where(pick, 1.0, 0.0).astype(BF16)
    slab[:SEL, :LANES] = mm(pick, k_turned).astype(BF16)
    slab[:SEL, LANES:] = mm(pick, values).astype(BF16)

    pl.semaphore_wait(barrier, n_kv - 1 + n_tp - 1)

    def slab_copy(slot, dst):
        return pltpu.make_async_remote_copy(
            src_ref=slab, dst_ref=gath.at[slot],
            send_sem=slab_ss.at[dst], recv_sem=slab_rs.at[slot],
            device_id={"kv": dst}, device_id_type=MESH,
        )

    def send_slab(i, carry):
        slab_copy(me, n_kv - 1 - i).start()
        return carry

    lax.fori_loop(0, n_kv - 1 - me, send_slab, 0)

    loads[5].wait()
    lane = iota((rows, LANES), 1)
    q_raw = mm(tokens, wq[...]).astype(BF16).astype(F32)
    q_gain = tile_lanes(qgain_ref[...], heads)
    q_plain = unit_norm(q_raw, q_gain)
    q_turned = rotate(q_plain).astype(BF16).astype(F32)
    q_plain = q_plain.astype(F32)
    scale = head_size ** (-0.5)
    for source, target in ((q_plain, qp_heads), (q_turned, qt_heads)):
        for h in range(heads):
            group = h // per_group
            part = source[:, (h // 2) * LANES:(h // 2 + 1) * LANES] * scale
            if h % 2 != group % 2:
                part = pltpu.roll(part, half, 1)
            target[h] = jnp.where((lane // half) == group % 2, part, 0.0).astype(BF16)
    loads[6].wait()
    gate_all = jax.nn.sigmoid(mm_t(tokens, wg[...]))
    gate_cols = gate_all.shape[1]
    gate_pad = jnp.concatenate([gate_all, jnp.zeros((rows, LANES - gate_cols), F32)], axis=1)
    gates[...] = pltpu.roll(gate_pad, lax.rem(LANES - my_tp * 2 * heads, LANES), 1)

    def wait_slab(d, carry):
        slab_copy(d, me).wait_recv()
        return carry

    lax.fori_loop(0, me, wait_slab, 0)
    loads[7].wait()

    slab_devs = min(n_kv, 8)
    n_slabs = n_kv // slab_devs
    stacked = heads * chunk
    sel_lane = iota((chunk, slab_devs * SEL), 1)
    sel_row = iota((chunk, slab_devs * SEL), 0)
    span_lane = iota((chunk, n_kv * SPAN_PAD), 1)
    span_row = iota((chunk, n_kv * SPAN_PAD), 0)
    span_keys = gath[:, SEL:, :LANES].reshape(n_kv * SPAN_PAD, LANES)
    span_values = gath[:, SEL:, LANES:].reshape(n_kv * SPAN_PAD, LANES)
    span_id = (span_lane // SPAN_PAD) * spans_dev + span_lane % SPAN_PAD
    chunk_lane = iota((chunk, LANES), 1)

    def masked(scores, mask):
        cube = scores.reshape(heads, chunk, scores.shape[1])
        return jnp.where(mask[None], cube, big_negative).reshape(scores.shape)

    def attend(which, slot_rows):
        start = pl.multiple_of(which * chunk, chunk)
        local_block = start // SEL
        block_start = pl.multiple_of(local_block * SEL, SEL)
        in_block = start - block_start
        gath[me, :SEL, :] = own[pl.ds(block_start, SEL), :]

        qp = qp_heads[:, pl.ds(start, chunk), :].reshape(stacked, LANES)
        qt = qt_heads[:, pl.ds(start, chunk), :].reshape(stacked, LANES)

        place = me * rows + start + span_row
        allowed = (span_lane % SPAN_PAD < spans_dev) & (span_id * CMP + CMP - 1 <= place)
        s = masked(mm_t(qp, span_keys), allowed)
        span_peak = jnp.max(s, axis=1, keepdims=True)
        w = jnp.exp(s - span_peak)
        span_sum = jnp.sum(w, axis=1, keepdims=True)
        span_out = mm(w.astype(BF16), span_values)

        def slab_step(i, carry):
            base_dev = i * slab_devs
            keys = gath[pl.ds(base_dev, slab_devs), :SEL, :LANES].reshape(slab_devs * SEL, LANES)
            vals = gath[pl.ds(base_dev, slab_devs), :SEL, LANES:].reshape(slab_devs * SEL, LANES)
            dev = base_dev + sel_lane // SEL
            member = dev == chosen_ref[local_block, 0]
            for j in range(1, n_chosen):
                member = member | (dev == chosen_ref[local_block, j])
            ok = (member & (dev < me)) | ((dev == me) & (sel_lane % SEL <= sel_row + in_block))
            sc = masked(mm_t(qt, keys), ok)
            peak = jnp.max(sc, axis=1, keepdims=True)
            if carry is None:
                e = jnp.exp(sc - peak)
                return peak, jnp.sum(e, axis=1, keepdims=True), mm(e.astype(BF16), vals)
            old_peak, old_sum, old_out = carry
            peak = jnp.maximum(peak, old_peak)
            factor = jnp.exp(old_peak - peak)
            e = jnp.exp(sc - peak) * jnp.where(sc > 0.5 * big_negative, 1.0, 0.0)
            return (
                peak,
                old_sum * factor + jnp.sum(e, axis=1, keepdims=True),
                old_out * factor + mm(e.astype(BF16), vals),
            )

        if n_slabs == 1:
            sel_peak, sel_sum, sel_out = slab_step(0, None)
        else:
            sel_peak, sel_sum, sel_out = lax.fori_loop(
                0, n_slabs, slab_step,
                (
                    jnp.full((stacked, 1), big_negative, F32),
                    jnp.zeros((stacked, 1), F32),
                    jnp.zeros((stacked, LANES), F32),
                ),
            )

        has_span = (me * rows + start + iota((chunk, 1), 0)) >= CMP - 1
        gate = gates[pl.ds(start, chunk), :]
        lse0 = jnp.zeros((chunk, LANES), F32)
        lse1 = jnp.zeros((chunk, LANES), F32)
        even = None
        for h in range(heads):
            piece = slice(h * chunk, (h + 1) * chunk)
            ssum = jnp.where(has_span, span_sum[piece], 1.0)
            g0 = jnp.where(has_span, gate[:, 2 * h:2 * h + 1] / ssum, 0.0)
            g1 = gate[:, 2 * h + 1:2 * h + 2] / sel_sum[piece]
            l0 = jnp.where(has_span, span_peak[piece] + jnp.log(ssum), 0.0)
            l1 = sel_peak[piece] + jnp.log(sel_sum[piece])
            lse0 = jnp.where(chunk_lane == h, l0, lse0)
            lse1 = jnp.where(chunk_lane == h, l1, lse1)
            both = g0 * span_out[piece] + g1 * sel_out[piece]
            if h % 2 != (h // per_group) % 2:
                both = pltpu.roll(both, half, 1)
            if h % 2 == 0:
                even = both
            else:
                pair = jnp.where(chunk_lane < half, even, both).astype(BF16)
                mixed[slot_rows:slot_rows + chunk, (h // 2) * LANES:(h // 2 + 1) * LANES] = pair
        lse_rows[0, pl.ds(start, chunk), :] = lse0
        lse_rows[1, pl.ds(start, chunk), :] = lse1

    def pair_copy(t):
        return pltpu.make_async_remote_copy(
            src_ref=pair_send.at[t], dst_ref=pair_recv.at[t],
            send_sem=pair_ss.at[t], recv_sem=pair_rs.at[t],
            device_id={"tp": my_x * 2 + 1 - my_core}, device_id_type=MESH,
        )

    def cross_copy(t):
        return pltpu.make_async_remote_copy(
            src_ref=cross_send.at[t - 1], dst_ref=cross_recv.at[t - 1],
            send_sem=cross_ss.at[t - 1], recv_sem=cross_rs.at[t - 1],
            device_id={"tp": lax.rem(my_x + t, n_x) * 2 + my_core}, device_id_type=MESH,
        )

    for t in range(n_x - 1, -1, -1):
        chip = lax.rem(my_x + t, n_x)
        attend(chip * 2 + 1 - my_core, 0)
        attend(chip * 2 + my_core, chunk)
        partial = mm(mixed[...], wo[...])
        pair_send[t] = partial[:chunk].astype(BF16)
        pair_copy(t).start()
        mine = partial[chunk:]
        pair_copy(t).wait_recv()
        mine = mine + pair_recv[t].astype(F32)
        if t > 0:
            cross_send[t - 1] = mine.astype(BF16)
            cross_copy(t).start()
        else:
            for u in range(n_x - 1, 0, -1):
                cross_copy(u).wait_recv()
                mine = mine + cross_recv[u - 1].astype(F32)
            out_ref[...] = mine.astype(BF16)
            for b in range(2):
                lse_ref[b] = jnp.transpose(lse_rows[b])[:heads]

    for t in range(n_x):
        pair_copy(t).wait_send()
        if t > 0:
            cross_copy(t).wait_send()

    def wait_sent(i, carry):
        slab_copy(me, n_kv - 1 - i).wait_send()
        return carry

    lax.fori_loop(0, n_kv - 1 - me, wait_sent, 0)


def rope_tables(rows, n_kv, head_size):
    inverse = np.power(rope_base, -np.arange(head_size // 2, dtype=np.float64) * 2.0 / head_size)
    inverse = np.tile(inverse, LANES // (head_size // 2))[None, :]
    near = np.arange(rows, dtype=np.float64)[:, None] * inverse
    far = np.arange(n_kv, dtype=np.float64)[:, None] * rows * inverse
    stack = lambda a: np.stack([np.cos(a), np.sin(a)]).astype(np.float32)
    return stack(near), stack(far)


def shards(
    n_kv, n_tp,
    tokens, query_weight, key_weight, value_weight, gate_weight,
    query_gain, key_gain, out_weight, shared_block, chosen_device,
):
    rows, width = tokens.shape
    head_size = query_gain.shape[0]
    heads = query_weight.shape[1] // head_size
    group_width = key_weight.shape[1]
    groups = group_width // head_size
    if group_width < LANES:
        pad = ((0, 0), (0, LANES - group_width))
        key_weight = jnp.pad(key_weight, pad)
        value_weight = jnp.pad(value_weight, pad)
    n_x = n_tp // 2
    chunk = rows // n_tp
    inner = heads * head_size
    d_out = out_weight.shape[1]
    near, far = rope_tables(rows, n_kv, head_size)
    hbm = pl.BlockSpec(memory_space=pl.ANY)
    vmem = pl.BlockSpec(memory_space=pltpu.VMEM)
    smem = pl.BlockSpec(memory_space=pltpu.SMEM)
    dma = pltpu.SemaphoreType.DMA
    mixed_out, lse = pl.pallas_call(
        functools.partial(layer_kernel, n_kv, n_tp, heads, groups, head_size),
        out_shape=(
            jax.ShapeDtypeStruct((chunk, d_out), BF16),
            jax.ShapeDtypeStruct((2, heads, rows), F32),
        ),
        in_specs=[hbm] * 8 + [vmem] * 2 + [smem] * 2,
        out_specs=(vmem, vmem),
        scratch_shapes=[
            pltpu.VMEM((rows, width), BF16),
            pltpu.VMEM((width, inner), BF16),
            pltpu.VMEM((width, 2 * LANES), BF16),
            pltpu.VMEM(gate_weight.shape[::-1], BF16),
            pltpu.VMEM((inner, d_out), BF16),
            pltpu.VMEM(near.shape, F32),
            pltpu.VMEM(far.shape, F32),
            pltpu.VMEM((rows, 2 * LANES), BF16),
            pltpu.VMEM((SEL + SPAN_PAD, 2 * LANES), BF16),
            pltpu.VMEM((n_kv, SEL + SPAN_PAD, 2 * LANES), BF16),
            pltpu.VMEM((heads, rows, LANES), BF16),
            pltpu.VMEM((heads, rows, LANES), BF16),
            pltpu.VMEM((rows, LANES), F32),
            pltpu.VMEM((2 * chunk, inner), BF16),
            pltpu.VMEM((2, rows, LANES), F32),
            pltpu.VMEM((n_x, chunk, d_out), BF16),
            pltpu.VMEM((n_x, chunk, d_out), BF16),
            pltpu.VMEM((n_x - 1, chunk, d_out), BF16),
            pltpu.VMEM((n_x - 1, chunk, d_out), BF16),
            dma((8,)),
            dma((n_kv,)),
            dma((n_kv,)),
            dma((n_x,)),
            dma((n_x,)),
            dma((n_x - 1,)),
            dma((n_x - 1,)),
        ],
        compiler_params=pltpu.CompilerParams(
            collective_id=0, has_side_effects=True, vmem_limit_bytes=60 * 1024 * 1024
        ),
        name="layer",
    )(
        tokens, query_weight, key_weight, value_weight, gate_weight.T, out_weight,
        jnp.asarray(near), jnp.asarray(far),
        query_gain.reshape(1, head_size), key_gain.reshape(1, head_size),
        shared_block, chosen_device,
    )
    return mixed_out, jnp.transpose(lse, (0, 2, 1))


def solution(mesh):
    placed = (
        P("kv", None),
        P(None, "tp"),
        P(None, "tp"),
        P(None, "tp"),
        P(),
        P(),
        P(),
        P("tp", None),
        P("kv"),
        P("kv", None),
    )
    return jax.shard_map(
        functools.partial(shards, mesh.shape["kv"], mesh.shape["tp"]),
        mesh=mesh,
        in_specs=placed,
        out_specs=(P(("kv", "tp"), None), P(None, "kv", "tp")),
        check_vma=False,
    )
```

time: 155 us -> 30.2 us (0.19); the launches traced: 152 us -> 30 us
  blocking collectives: 44.6 us -> 0 us
  waiting for transfers between devices: 41.6 us -> 0 us
  Pallas kernels: 0 us -> 25.7 us
  local copies, waits for them, and re-layouts: 23.8 us -> 2.99 us
  between operations: 15.2 us -> 1.29 us
  matrix products: 13.5 us -> 0 us
  other arithmetic: 13.2 us -> 0 us
    all_gather x2 -> x0, blocking collectives: 44.6 us -> none  [the longest x1 23.9 us: shards(): all_summary = lax.all_gather(summary, 'kv', axis=0, tiled=True)]
    reduce_scatter x1 -> x0, waiting for transfers between devices: 41.5 us -> none  [shards(): lax.psum_scatter(jnp.dot(mixed_heads, out_weight, preferred_element_type=...]
    pallas_call x0 -> x1, Pallas kernels: none -> 25.7 us  [shards(): pl.pallas_call(functools.partial(layer_kernel, n_kv, n_tp, heads, groups,...]
    dot_general x11 -> x0, matrix products: 13.5 us -> none  [the longest x1 2.3 us: shards(): jnp.dot(tokens, query_weight, preferred_element_type=jnp.float32)]
    concatenate x8 -> x0, local copies, waits for them, and re-layouts: 9.29 us -> none  [rotate(): jnp.concatenate([front_half * cos_vals - back_half * sin_vals, back_half...]
    reshape x6 -> x0, local copies, waits for them, and re-layouts: 6.32 us -> none  [the longest x2 4.33 us: shards(): chosen_out.reshape(tok_rows, head_count, head_size)]
    convert_element_type x8 -> x0, other arithmetic: 4.45 us -> none  [the longest x2 1.88 us: rounded(): return lax.optimization_barrier(values_in.astype(jnp.bfloat16))]
    slice x6 -> x0, local copies, waits for them, and re-layouts: 3.52 us -> none  [the longest x2 2.38 us: absorb_slab(): slab_values = slab_rows[:, group_width:].reshape(-1, groups, head_size)]
  transfers between devices with their start and end apart: 1 -> 0, of which waited for: 1 -> 0; matrix products, arithmetic and copies ran while one was open for 1% -> 0% of each run, Pallas kernels for 0% -> 0%
where the time goes in v1:
time: 30.2 us; the launch traced here: 30 us
  Pallas kernels  25.7 us (85%)
  local copies, waits for them, and re-layouts  2.99 us (10%)
  between operations  1.29 us (4%)
    pallas_call x1, Pallas kernels, shards(): pl.pallas_call(functools.partial(layer_kernel, n_kv, n_tp, heads, groups,...  25.7 us
    unnamed x2, local copies, waits for them, and re-layouts  2.99 us

profile of v1, /device:TPU:17, one launch (start us, length us, event | category | flops | bytes accessed | tf_op | source)
XLA Modules:
  0.0 30.0 jit_solution(10002688546536634495)
XLA Ops:
  1.3 25.7 %layer.1 = (bf16[64,2048]{1,0:T(8,128)(2,1)}, f32[2,8,256]{2,1,0:T(8,128)}) custom-call(bf16[256,2048]{1,0:T(8,128)(2,1)} %tok_hbm.1, bf16[2048,512]{1,0:T(8,128)(2,1)} %wq_hbm.1, bf16[2048,128]{1,0:T(8,128)(2,1)} %wk_hbm.1, bf16[2048,128]{1,0:T(8,128)(2,1)} %wv_hbm.1, bf16[64,2048]{1,0:T(8,128)(2,1)} %bitcast.4, bf16[512,2048]{1,0:T(8,128)(2,1)} %wo_hbm.1, ...), custom_call_target="tpu_custom_call" | custom-call | tf_op jit(solution)/shard_map/layer/pallas_call | solution.py:375
  27.0 1.7 %copy.17 = bf16[64,2048]{1,0:T(8,128)(2,1)} copy(bf16[64,2048]{1,0:T(8,128)(2,1)} %get-tuple-element.8) | data formatting | bytes 524288
  28.6 1.3 %copy.18 = f32[2,256,8]{1,2,0:T(8,128)} copy(f32[2,256,8]{1,2,0:T(8,128)} %bitcast.5) | data formatting | bytes 32768

commit v2 on v1

--- a/solution.py
+++ b/solution.py
@@ -375,8 +375,8 @@
     mixed_out, lse = pl.pallas_call(
         functools.partial(layer_kernel, n_kv, n_tp, heads, groups, head_size),
         out_shape=(
-            jax.ShapeDtypeStruct((chunk, d_out), BF16),
-            jax.ShapeDtypeStruct((2, heads, rows), F32),
+            pltpu.VMEM((chunk, d_out), BF16),
+            pltpu.VMEM((2, heads, rows), F32),
         ),
         in_specs=[hbm] * 8 + [vmem] * 2 + [smem] * 2,
         out_specs=(vmem, vmem),

time: 30.2 us -> 27.8 us (0.921)
  local copies, waits for them, and re-layouts: 2.99 us -> 1.31 us
  Pallas kernels: 25.7 us -> 25 us
    unnamed x2, local copies, waits for them, and re-layouts: 2.99 us -> 1.31 us
    pallas_call x1, Pallas kernels: 25.7 us -> 25 us  [shards(): pl.pallas_call(functools.partial(layer_kernel, n_kv, n_tp, heads, groups,...]
where the time goes in v2:
time: 27.8 us; the launch traced here: 27.6 us
  Pallas kernels  25 us (90%)
  local copies, waits for them, and re-layouts  1.31 us (5%)
  between operations  1.29 us (5%)
    pallas_call x1, Pallas kernels, shards(): pl.pallas_call(functools.partial(layer_kernel, n_kv, n_tp, heads, groups,...  25 us
    unnamed x2, local copies, waits for them, and re-layouts  1.31 us

profile of v2, /device:TPU:17, one launch (start us, length us, event | category | flops | bytes accessed | tf_op | source)
XLA Modules:
  0.0 27.6 jit_solution(11984078243346242065)
XLA Ops:
  1.3 25.0 %layer.1 = (bf16[64,2048]{1,0:T(8,128)(2,1)S(1)}, f32[2,8,256]{2,1,0:T(8,128)S(1)}) custom-call(bf16[256,2048]{1,0:T(8,128)(2,1)} %tok_hbm.1, bf16[2048,512]{1,0:T(8,128)(2,1)} %wq_hbm.1, bf16[2048,128]{1,0:T(8,128)(2,1)} %wk_hbm.1, bf16[2048,128]{1,0:T(8,128)(2,1)} %wv_hbm.1, bf16[64,2048]{1,0:T(8,128)(2,1)} %bitcast.5, bf16[512,2048]{1,0:T(8,128)(2,1)} %wo_hbm.1, ...), custom_call_target="tpu_custom_call" | custom-call | tf_op jit(solution)/shard_map/layer/pallas_call | solution.py:375
  26.3 0.7 %copy.16 = bf16[64,2048]{1,0:T(8,128)(2,1)} copy(bf16[64,2048]{1,0:T(8,128)(2,1)S(1)} %get-tuple-element.6) | data formatting | bytes 524288
  27.0 0.6 %copy.17 = f32[2,256,8]{1,2,0:T(8,128)} copy(f32[2,256,8]{1,2,0:T(8,128)S(1)} %bitcast.4) | data formatting | bytes 32768

commit v3 on v2

--- a/solution.py
+++ b/solution.py
@@ -12,6 +12,7 @@
 CMP = 32
 LANES = 128
 SPAN_PAD = 16
+PIECES = 2
 
 norm_eps = 1e-06
 rope_base = 500000.0
@@ -52,7 +53,7 @@
     per_group = heads // groups
     half = LANES // 2
     n_x = n_tp // 2
-    chunk = rows // n_tp
+    rows_out = rows // n_tp
     n_chosen = chosen_ref.shape[1]
     me = lax.axis_index("kv")
     my_tp = lax.axis_index("tp")
@@ -165,7 +166,7 @@
         )
 
     def send_slab(i, carry):
-        slab_copy(me, n_kv - 1 - i).start()
+        slab_copy(me, me + 1 + i).start()
         return carry
 
     lax.fori_loop(0, n_kv - 1 - me, send_slab, 0)
@@ -186,10 +187,12 @@
                 part = pltpu.roll(part, half, 1)
             target[h] = jnp.where((lane // half) == group % 2, part, 0.0).astype(BF16)
     loads[6].wait()
-    gate_all = jax.nn.sigmoid(mm_t(tokens, wg[...]))
-    gate_cols = gate_all.shape[1]
-    gate_pad = jnp.concatenate([gate_all, jnp.zeros((rows, LANES - gate_cols), F32)], axis=1)
-    gates[...] = pltpu.roll(gate_pad, lax.rem(LANES - my_tp * 2 * heads, LANES), 1)
+    pick_row = iota((2 * LANES, wg.shape[0]), 0)
+    pick_head = pick_row % LANES
+    pick_col = 2 * (my_tp * heads + pick_head) + pick_row // LANES
+    pick_gate = (pick_head < heads) & (iota((2 * LANES, wg.shape[0]), 1) == pick_col)
+    gate_weights = mm(jnp.where(pick_gate, 1.0, 0.0).astype(BF16), wg[...]).astype(BF16)
+    gates[...] = jax.nn.sigmoid(mm_t(tokens, gate_weights))
 
     def wait_slab(d, carry):
         slab_copy(d, me).wait_recv()
@@ -200,22 +203,22 @@
 
     slab_devs = min(n_kv, 8)
     n_slabs = n_kv // slab_devs
-    stacked = heads * chunk
-    sel_lane = iota((chunk, slab_devs * SEL), 1)
-    sel_row = iota((chunk, slab_devs * SEL), 0)
-    span_lane = iota((chunk, n_kv * SPAN_PAD), 1)
-    span_row = iota((chunk, n_kv * SPAN_PAD), 0)
     span_keys = gath[:, SEL:, :LANES].reshape(n_kv * SPAN_PAD, LANES)
     span_values = gath[:, SEL:, LANES:].reshape(n_kv * SPAN_PAD, LANES)
-    span_id = (span_lane // SPAN_PAD) * spans_dev + span_lane % SPAN_PAD
-    chunk_lane = iota((chunk, LANES), 1)
-
-    def masked(scores, mask):
-        cube = scores.reshape(heads, chunk, scores.shape[1])
-        return jnp.where(mask[None], cube, big_negative).reshape(scores.shape)
-
-    def attend(which, slot_rows):
-        start = pl.multiple_of(which * chunk, chunk)
+    def attend(which, offset, chunk):
+        stacked = heads * chunk
+        sel_lane = iota((chunk, slab_devs * SEL), 1)
+        sel_row = iota((chunk, slab_devs * SEL), 0)
+        span_lane = iota((chunk, n_kv * SPAN_PAD), 1)
+        span_row = iota((chunk, n_kv * SPAN_PAD), 0)
+        span_id = (span_lane // SPAN_PAD) * spans_dev + span_lane % SPAN_PAD
+        chunk_lane = iota((chunk, LANES), 1)
+
+        def masked(scores, mask):
+            cube = scores.reshape(heads, chunk, scores.shape[1])
+            return jnp.where(mask[None], cube, big_negative).reshape(scores.shape)
+
+        start = pl.multiple_of(which * rows_out + offset, chunk)
         local_block = start // SEL
         block_start = pl.multiple_of(local_block * SEL, SEL)
         in_block = start - block_start
@@ -268,70 +271,81 @@
                 ),
             )
 
-        has_span = (me * rows + start + iota((chunk, 1), 0)) >= CMP - 1
+        def by_head(column):
+            acc = jnp.zeros((chunk, LANES), F32)
+            for h in range(heads):
+                acc = jnp.where(chunk_lane == h, column[h * chunk:(h + 1) * chunk], acc)
+            return acc
+
+        has_span = (me * rows + start + iota((chunk, LANES), 0)) >= CMP - 1
+        valid = chunk_lane < heads
+        ssum = jnp.where(has_span & valid, by_head(span_sum), 1.0)
+        lsum = jnp.where(valid, by_head(sel_sum), 1.0)
         gate = gates[pl.ds(start, chunk), :]
-        lse0 = jnp.zeros((chunk, LANES), F32)
-        lse1 = jnp.zeros((chunk, LANES), F32)
+        g0 = jnp.where(has_span, gate[:, :LANES] / ssum, 0.0)
+        g1 = gate[:, LANES:] / lsum
         even = None
         for h in range(heads):
             piece = slice(h * chunk, (h + 1) * chunk)
-            ssum = jnp.where(has_span, span_sum[piece], 1.0)
-            g0 = jnp.where(has_span, gate[:, 2 * h:2 * h + 1] / ssum, 0.0)
-            g1 = gate[:, 2 * h + 1:2 * h + 2] / sel_sum[piece]
-            l0 = jnp.where(has_span, span_peak[piece] + jnp.log(ssum), 0.0)
-            l1 = sel_peak[piece] + jnp.log(sel_sum[piece])
-            lse0 = jnp.where(chunk_lane == h, l0, lse0)
-            lse1 = jnp.where(chunk_lane == h, l1, lse1)
-            both = g0 * span_out[piece] + g1 * sel_out[piece]
+            both = g0[:, h:h + 1] * span_out[piece] + g1[:, h:h + 1] * sel_out[piece]
             if h % 2 != (h // per_group) % 2:
                 both = pltpu.roll(both, half, 1)
             if h % 2 == 0:
                 even = both
             else:
                 pair = jnp.where(chunk_lane < half, even, both).astype(BF16)
-                mixed[slot_rows:slot_rows + chunk, (h // 2) * LANES:(h // 2 + 1) * LANES] = pair
-        lse_rows[0, pl.ds(start, chunk), :] = lse0
-        lse_rows[1, pl.ds(start, chunk), :] = lse1
-
-    def pair_copy(t):
+                mixed[:chunk, (h // 2) * LANES:(h // 2 + 1) * LANES] = pair
+        lse_rows[0, pl.ds(start, chunk), :] = jnp.where(has_span, by_head(span_peak) + jnp.log(ssum), 0.0)
+        lse_rows[1, pl.ds(start, chunk), :] = by_head(sel_peak) + jnp.log(lsum)
+
+    sub = rows_out // PIECES
+
+    def pair_copy(t, p, n):
+        part = pl.ds(p * sub, n)
         return pltpu.make_async_remote_copy(
-            src_ref=pair_send.at[t], dst_ref=pair_recv.at[t],
-            send_sem=pair_ss.at[t], recv_sem=pair_rs.at[t],
+            src_ref=pair_send.at[t, part], dst_ref=pair_recv.at[t, part],
+            send_sem=pair_ss.at[t, p], recv_sem=pair_rs.at[t, p],
             device_id={"tp": my_x * 2 + 1 - my_core}, device_id_type=MESH,
         )
 
-    def cross_copy(t):
+    def cross_copy(t, p):
         return pltpu.make_async_remote_copy(
-            src_ref=cross_send.at[t - 1], dst_ref=cross_recv.at[t - 1],
-            send_sem=cross_ss.at[t - 1], recv_sem=cross_rs.at[t - 1],
+            src_ref=cross_send.at[t - 1, p], dst_ref=cross_recv.at[t - 1, p],
+            send_sem=cross_ss.at[t - 1, p], recv_sem=cross_rs.at[t - 1, p],
             device_id={"tp": lax.rem(my_x + t, n_x) * 2 + my_core}, device_id_type=MESH,
         )
 
     for t in range(n_x - 1, -1, -1):
         chip = lax.rem(my_x + t, n_x)
-        attend(chip * 2 + 1 - my_core, 0)
-        attend(chip * 2 + my_core, chunk)
-        partial = mm(mixed[...], wo[...])
-        pair_send[t] = partial[:chunk].astype(BF16)
-        pair_copy(t).start()
-        mine = partial[chunk:]
-        pair_copy(t).wait_recv()
-        mine = mine + pair_recv[t].astype(F32)
-        if t > 0:
-            cross_send[t - 1] = mine.astype(BF16)
-            cross_copy(t).start()
-        else:
-            for u in range(n_x - 1, 0, -1):
-                cross_copy(u).wait_recv()
-                mine = mine + cross_recv[u - 1].astype(F32)
-            out_ref[...] = mine.astype(BF16)
-            for b in range(2):
-                lse_ref[b] = jnp.transpose(lse_rows[b])[:heads]
+        pieces = PIECES if t > 0 else 1
+        n = rows_out // pieces
+        for p in range(pieces):
+            part = slice(p * n, (p + 1) * n)
+            attend(chip * 2 + 1 - my_core, p * n, n)
+            pair_send[t, part] = mm(mixed[:n], wo[...]).astype(BF16)
+            pair_copy(t, p, n).start()
+            attend(chip * 2 + my_core, p * n, n)
+            mine = mm(mixed[:n], wo[...])
+            pair_copy(t, p, n).wait_recv()
+            mine = mine + pair_recv[t, part].astype(F32)
+            if t > 0:
+                cross_send[t - 1, p] = mine.astype(BF16)
+                cross_copy(t, p).start()
+    for b in range(2):
+        lse_ref[b] = jnp.transpose(lse_rows[b])[:heads]
+    for p in range(PIECES):
+        part = mine[p * sub:(p + 1) * sub]
+        for u in range(n_x - 1, 0, -1):
+            cross_copy(u, p).wait_recv()
+            part = part + cross_recv[u - 1, p].astype(F32)
+        out_ref[p * sub:(p + 1) * sub] = part.astype(BF16)
 
     for t in range(n_x):
-        pair_copy(t).wait_send()
-        if t > 0:
-            cross_copy(t).wait_send()
+        pieces = PIECES if t > 0 else 1
+        for p in range(pieces):
+            pair_copy(t, p, rows_out // pieces).wait_send()
+            if t > 0:
+                cross_copy(t, p).wait_send()
 
     def wait_sent(i, carry):
         slab_copy(me, n_kv - 1 - i).wait_send()
@@ -393,20 +407,20 @@
             pltpu.VMEM((n_kv, SEL + SPAN_PAD, 2 * LANES), BF16),
             pltpu.VMEM((heads, rows, LANES), BF16),
             pltpu.VMEM((heads, rows, LANES), BF16),
-            pltpu.VMEM((rows, LANES), F32),
-            pltpu.VMEM((2 * chunk, inner), BF16),
+            pltpu.VMEM((rows, 2 * LANES), F32),
+            pltpu.VMEM((chunk, inner), BF16),
             pltpu.VMEM((2, rows, LANES), F32),
             pltpu.VMEM((n_x, chunk, d_out), BF16),
             pltpu.VMEM((n_x, chunk, d_out), BF16),
-            pltpu.VMEM((n_x - 1, chunk, d_out), BF16),
-            pltpu.VMEM((n_x - 1, chunk, d_out), BF16),
+            pltpu.VMEM((n_x - 1, PIECES, chunk // PIECES, d_out), BF16),
+            pltpu.VMEM((n_x - 1, PIECES, chunk // PIECES, d_out), BF16),
             dma((8,)),
             dma((n_kv,)),
             dma((n_kv,)),
-            dma((n_x,)),
-            dma((n_x,)),
-            dma((n_x - 1,)),
-            dma((n_x - 1,)),
+            dma((n_x, PIECES)),
+            dma((n_x, PIECES)),
+            dma((n_x - 1, PIECES)),
+            dma((n_x - 1, PIECES)),
         ],
         compiler_params=pltpu.CompilerParams(
             collective_id=0, has_side_effects=True, vmem_limit_bytes=60 * 1024 * 1024

time: 27.8 us -> 26.5 us (0.953)
  the two profiles are of different devices: /device:TPU:17 before, /device:TPU:24 now
where the time goes in v3:
time: 26.5 us; the launch traced here: 26.3 us
  Pallas kernels  23.7 us (89%)
  local copies, waits for them, and re-layouts  1.31 us (5%)
  between operations  1.29 us (5%)
    pallas_call x1, Pallas kernels, shards(): pl.pallas_call(functools.partial(layer_kernel, n_kv, n_tp, heads, groups,...  23.7 us
    unnamed x2, local copies, waits for them, and re-layouts  1.31 us

profile of v3, /device:TPU:24, one launch (start us, length us, event | category | flops | bytes accessed | tf_op | source)
XLA Modules:
  0.0 26.3 jit_solution(4568764496466362294)
XLA Ops:
  1.3 23.7 %layer.1 = (bf16[64,2048]{1,0:T(8,128)(2,1)S(1)}, f32[2,8,256]{2,1,0:T(8,128)S(1)}) custom-call(bf16[256,2048]{1,0:T(8,128)(2,1)} %tok_hbm.1, bf16[2048,512]{1,0:T(8,128)(2,1)} %wq_hbm.1, bf16[2048,128]{1,0:T(8,128)(2,1)} %wk_hbm.1, bf16[2048,128]{1,0:T(8,128)(2,1)} %wv_hbm.1, bf16[64,2048]{1,0:T(8,128)(2,1)} %bitcast.5, bf16[512,2048]{1,0:T(8,128)(2,1)} %wo_hbm.1, ...), custom_call_target="tpu_custom_call" | custom-call | tf_op jit(solution)/shard_map/layer/pallas_call | solution.py:389
  25.0 0.7 %copy.16 = bf16[64,2048]{1,0:T(8,128)(2,1)} copy(bf16[64,2048]{1,0:T(8,128)(2,1)S(1)} %get-tuple-element.6) | data formatting | bytes 524288
  25.7 0.6 %copy.17 = f32[2,256,8]{1,2,0:T(8,128)} copy(f32[2,256,8]{1,2,0:T(8,128)S(1)} %bitcast.4) | data formatting | bytes 32768
